TPU v7x, 32 devices: a whole 2x2x4 slice. The times are simulated.
32 devices in a mesh: dp: 4 (over y, x), kv: 4 (over z), tp: 2 (over core).
Axes of the slice: x: 2, y: 2, z: 4, core: 2. Of those that a mesh axis runs over, the one named last changes fastest.
Arguments:
- piece_tokens: bfloat16 [256, 2048], P(('dp', 'kv')), parts along dimension 0, may hold values from -6 to 6
- dec_tokens: bfloat16 [192, 4, 2048], P(('dp', 'kv')), parts along dimension 0, may hold values from -6 to 6
- norm_gain: float32 [2048], replicated, may hold values from 0.1 to 1.9
- query_weight: bfloat16 [2048, 1024], P(None, 'tp'), may hold values from -0.375 to 0.375
- key_weight: bfloat16 [2048, 256], P(None, 'tp'), may hold values from -0.125 to 0.125
- value_weight: bfloat16 [2048, 256], P(None, 'tp'), may hold values from -0.125 to 0.125
- gate_weight: bfloat16 [2048, 8], P(None, 'tp'), may hold values from -0.125 to 0.125
- gate_bias: float32 [8], P('tp'), may hold values from 3.4 to 11
- out_weight: bfloat16 [1024, 2048], P('tp'), may hold values from -0.1875 to 0.1875
- out_gain: float32 [2048], replicated, may hold values from 0.1 to 1.9
- past_keys: bfloat16 [4096, 2, 128], P(('dp', 'kv'), 'tp'), parts along dimension 0, may hold values from -41 to 41
- past_values: bfloat16 [4096, 2, 128], P(('dp', 'kv'), 'tp'), parts along dimension 0, may hold values from -6 to 6
- past_gate: float32 [8, 4096], P('tp', ('dp', 'kv')), parts along dimension 1, may hold values from -1024 to 0
- dec_keys: bfloat16 [192, 512, 2, 128], P(('dp', 'kv'), None, 'tp'), parts along dimension 0, may hold values from -41 to 41
- dec_values: bfloat16 [192, 512, 2, 128], P(('dp', 'kv'), None, 'tp'), parts along dimension 0, may hold values from -6 to 6
- dec_gate: float32 [192, 8, 512], P(('dp', 'kv'), 'tp'), parts along dimension 0, may hold values from -512 to 0
- dec_lengths: int32 [192], P(('dp', 'kv')), parts along dimension 0, may hold values from 1 to 512, as said below
Outputs:
- piece_out: bfloat16 [256, 2048], P(('dp', 'kv')), parts along dimension 0
- dec_out: bfloat16 [192, 4, 2048], P(('dp', 'kv')), parts along dimension 0
There are 4 independent parts, one for each index of `dp`. A program takes and returns all parts, laid end to end along the dimension named above; an argument that names none is the same for every part. Nothing has to cross between parts.
Inputs may be any that keep to these rules, and one draw needn't show every extreme that they name: `dec_lengths`: some decoding sequence has all 512 slots live in every draw.
All inputs are finite; a program needn't handle non-finite values.
Results may differ from a plain program's by a relative error of at most 0.015.
Values may be sent and summed in bfloat16 or wider, within the bound.
A program may use at most 64 MiB of HBM per device.

v0:
```python
import jax
import jax.numpy as jnp
from jax import lax
from jax.sharding import PartitionSpec as P

EPS = 1e-06


def rms_scale(source, scale_gain):
    widened = source.astype(jnp.float32)
    return (
        widened * lax.rsqrt(jnp.mean(widened * widened, axis=-1, keepdims=True) + EPS) * scale_gain
    )


def body(
    piece_tokens,
    dec_tokens,
    norm_gain,
    query_weight,
    key_weight,
    value_weight,
    gate_weight,
    gate_bias,
    out_weight,
    out_gain,
    past_keys,
    past_values,
    past_gate,
    dec_keys,
    dec_values,
    dec_gate,
    dec_lengths,
):
    piece_rows = piece_tokens.shape[0]
    model_width = piece_tokens.shape[1]
    kv_local = past_keys.shape[1]
    head_dim = past_keys.shape[2]
    heads_local = gate_bias.shape[0]
    group_size = heads_local // kv_local
    score_scale = head_dim ** (-0.5)
    seq_count = dec_tokens.shape[0]
    new_count = dec_tokens.shape[1]
    kv_count = lax.axis_size("kv")
    position = lax.axis_index("kv")
    all_rows = jnp.concatenate(
        [piece_tokens, dec_tokens.reshape(seq_count * new_count, model_width)], axis=0
    )
    normed = rms_scale(all_rows, norm_gain).astype(jnp.bfloat16)
    queries = jnp.dot(normed, query_weight, preferred_element_type=jnp.float32).astype(jnp.bfloat16)
    key_rows = jnp.dot(normed, key_weight, preferred_element_type=jnp.float32).astype(jnp.bfloat16)
    value_rows = jnp.dot(normed, value_weight, preferred_element_type=jnp.float32).astype(
        jnp.bfloat16
    )
    log_gates = jax.nn.log_sigmoid(
        jnp.dot(normed, gate_weight, preferred_element_type=jnp.float32) + gate_bias
    )
    piece_queries = queries[:piece_rows]
    piece_keys = key_rows[:piece_rows].reshape(piece_rows, kv_local, head_dim)
    piece_values = value_rows[:piece_rows].reshape(piece_rows, kv_local, head_dim)
    local_run = jnp.cumsum(log_gates[:piece_rows], axis=0)
    gathered_run = lax.all_gather(local_run, "kv", axis=0, tiled=True)
    shard_run = gathered_run.reshape(kv_count, piece_rows, heads_local)
    totals = shard_run[:, -1]
    before = jnp.cumsum(totals, axis=0) - totals
    piece_run = (shard_run + before[:, None, :]).reshape(kv_count * piece_rows, heads_local)
    own_run = lax.dynamic_slice_in_dim(piece_run, position * piece_rows, piece_rows, 0)
    key_place = position * piece_rows + jnp.arange(piece_rows)
    gate_groups = jnp.moveaxis(past_gate.reshape(kv_local, group_size, -1), 1, 0)
    own_groups = jnp.moveaxis(own_run.reshape(piece_rows, kv_local, group_size), 2, 0)
    shard_queries = lax.all_gather(piece_queries, "kv", axis=0, tiled=True)
    row_count = shard_queries.shape[0]
    query_groups = jnp.moveaxis(
        shard_queries.reshape(row_count, kv_local, group_size, head_dim), 2, 0
    )
    run_groups = jnp.moveaxis(piece_run.reshape(row_count, kv_local, group_size), 2, 0)
    row_place = jnp.arange(row_count)
    causal = key_place[None, :] <= row_place[:, None]

    def one_group(inputs):
        query_one, run_one, gate_one, key_run_one = inputs
        row_bias = run_one.T[:, :, None]
        past_scores = (
            jnp.einsum("nkd,pkd->knp", query_one, past_keys, preferred_element_type=jnp.float32)
            * score_scale
        )
        past_scores = past_scores + gate_one[:, None, :] + row_bias
        new_scores = (
            jnp.einsum("nkd,jkd->knj", query_one, piece_keys, preferred_element_type=jnp.float32)
            * score_scale
        )
        new_scores = new_scores + row_bias - key_run_one.T[:, None, :]
        new_scores = jnp.where(causal[None], new_scores, -jnp.inf)
        row_top = jnp.maximum(jnp.max(past_scores, axis=-1), jnp.max(new_scores, axis=-1))
        past_exp = jnp.exp(past_scores - row_top[..., None])
        new_exp = jnp.exp(new_scores - row_top[..., None])
        row_total = jnp.sum(past_exp, axis=-1) + jnp.sum(new_exp, axis=-1)
        summed = jnp.einsum(
            "knp,pkd->nkd",
            past_exp.astype(jnp.bfloat16),
            past_values,
            preferred_element_type=jnp.float32,
        )
        summed = summed + jnp.einsum(
            "knj,jkd->nkd",
            new_exp.astype(jnp.bfloat16),
            piece_values,
            preferred_element_type=jnp.float32,
        )
        return (summed, row_top.T, row_total.T)

    group_out, group_top, group_total = lax.map(
        one_group, (query_groups, run_groups, gate_groups, own_groups)
    )
    group_out = jnp.moveaxis(group_out, 0, 2).reshape(row_count, heads_local, head_dim)
    group_top = jnp.moveaxis(group_top, 0, 2).reshape(row_count, heads_local)
    group_total = jnp.moveaxis(group_total, 0, 2).reshape(row_count, heads_local)
    arrived = (
        lax.all_to_all(
            group_out.reshape(kv_count, piece_rows, heads_local, head_dim),
            "kv",
            split_axis=0,
            concat_axis=0,
            tiled=True,
        ),
        lax.all_to_all(
            group_top.reshape(kv_count, piece_rows, heads_local),
            "kv",
            split_axis=0,
            concat_axis=0,
            tiled=True,
        ),
        lax.all_to_all(
            group_total.reshape(kv_count, piece_rows, heads_local),
            "kv",
            split_axis=0,
            concat_axis=0,
            tiled=True,
        ),
    )
    global_top = jnp.max(arrived[1], axis=0)
    weights = jnp.exp(arrived[1] - global_top)
    row_total = jnp.sum(arrived[2] * weights, axis=0)
    piece_result = jnp.sum(arrived[0] * weights[..., None], axis=0) / row_total[..., None]
    piece_attention = piece_result.reshape(piece_rows, heads_local * head_dim).astype(jnp.bfloat16)
    dec_queries = queries[piece_rows:].reshape(seq_count, new_count, kv_local, group_size, head_dim)
    dec_new_keys = key_rows[piece_rows:].reshape(seq_count, new_count, kv_local, head_dim)
    dec_new_values = value_rows[piece_rows:].reshape(seq_count, new_count, kv_local, head_dim)
    dec_run = jnp.cumsum(log_gates[piece_rows:].reshape(seq_count, new_count, heads_local), axis=1)
    past_len = dec_keys.shape[1]
    slot_index = jnp.arange(past_len)
    last_gate = jnp.sum(
        jnp.where(slot_index[None, None, :] == (dec_lengths - 1)[:, None, None], dec_gate, 0.0),
        axis=2,
    )
    query_bias = jnp.moveaxis(dec_run.reshape(seq_count, new_count, kv_local, group_size), 1, 3)
    past_bias = last_gate.reshape(seq_count, kv_local, group_size)[..., None, None]
    dec_gate_groups = dec_gate.reshape(seq_count, kv_local, group_size, past_len)
    new_scores = (
        jnp.einsum(
            "stkgd,sukd->skgtu", dec_queries, dec_new_keys, preferred_element_type=jnp.float32
        )
        * score_scale
    )
    new_scores = new_scores + query_bias[..., None] - query_bias[..., None, :]
    new_causal = jnp.arange(new_count)[None, :] <= jnp.arange(new_count)[:, None]
    new_scores = jnp.where(new_causal, new_scores, -jnp.inf)
    new_top = jnp.max(new_scores, axis=-1)
    new_exp = jnp.exp(new_scores - new_top[..., None])
    start_dec = (
        jnp.einsum(
            "skgtu,sukd->skgtd",
            new_exp.astype(jnp.bfloat16),
            dec_new_values,
            preferred_element_type=jnp.float32,
        ),
        new_top,
        jnp.sum(new_exp, axis=-1),
    )
    block_scores = (
        jnp.einsum("stkgd,spkd->skgtp", dec_queries, dec_keys, preferred_element_type=jnp.float32)
        * score_scale
    )
    block_scores = (
        block_scores + query_bias[..., None] + past_bias - dec_gate_groups[:, :, :, None, :]
    )
    live_mask = jnp.arange(past_len)[None, :] < dec_lengths[:, None]
    block_scores = jnp.where(live_mask[:, None, None, None, :], block_scores, -jnp.inf)
    row_top = jnp.maximum(start_dec[1], jnp.max(block_scores, axis=-1))
    block_exp = jnp.exp(block_scores - row_top[..., None])
    rescale = jnp.exp(start_dec[1] - row_top)
    summed = start_dec[0] * rescale[..., None] + jnp.einsum(
        "skgtp,spkd->skgtd",
        block_exp.astype(jnp.bfloat16),
        dec_values,
        preferred_element_type=jnp.float32,
    )
    dec_attention = summed / (start_dec[2] * rescale + jnp.sum(block_exp, axis=-1))[..., None]
    dec_attention = (
        jnp.transpose(dec_attention, (0, 3, 1, 2, 4))
        .reshape(seq_count * new_count, heads_local * head_dim)
        .astype(jnp.bfloat16)
    )
    attention = jnp.concatenate([piece_attention, dec_attention], axis=0)
    partial_rows = jnp.dot(attention, out_weight, preferred_element_type=jnp.float32)
    mixed = lax.psum(partial_rows.astype(jnp.bfloat16), "tp").astype(jnp.float32)
    final_rows = rms_scale(mixed, out_gain).astype(jnp.bfloat16)
    return (
        final_rows[:piece_rows],
        final_rows[piece_rows:].reshape(seq_count, new_count, model_width),
    )


def solution(mesh):
    return jax.shard_map(
        body,
        mesh=mesh,
        in_specs=(
            P(("dp", "kv"), None),
            P(("dp", "kv"), None, None),
            P(),
            P(None, "tp"),
            P(None, "tp"),
            P(None, "tp"),
            P(None, "tp"),
            P("tp"),
            P("tp", None),
            P(),
            P(("dp", "kv"), "tp", None),
            P(("dp", "kv"), "tp", None),
            P("tp", ("dp", "kv")),
            P(("dp", "kv"), None, "tp", None),
            P(("dp", "kv"), None, "tp", None),
            P(("dp", "kv"), "tp", None),
            P(("dp", "kv")),
        ),
        out_specs=(P(("dp", "kv"), None), P(("dp", "kv"), None, None)),
        check_vma=False,
    )
```

profile of v0, /device:TPU:0, one launch (start us, length us, event | category | flops | bytes accessed | tf_op | source)
XLA Modules:
  0.0 105.0 jit_solution(5508176570152350641)
XLA Ops:
  7.2 1.1 %reshape.318 = bf16[48,2048]{1,0:T(8,128)(2,1)S(1)} reshape(bf16[12,4,2048]{2,1,0:T(4,128)(2,1)} %param.20) | data formatting | bytes 393216 | tf_op jit(solution)/shard_map/reshape | solution.py:47
  8.4 1.0 fusion.69
  9.4 1.1 %fusion.87 = f32[64,4]{0,1:T(4,128)S(1)} fusion(bf16[2048,4]{0,1:T(4,128)(2,1)} %param.25, f32[4]{0:T(128)} %param.26, f32[2048]{0:T(1024)} %param.21, f32[64]{0:T(128)S(1)} %add_rsqrt_fusion.1, bf16[48,2048]{1,0:T(8,128)(2,1)S(1)} %reshape.318, bf16[16,2048]{1,0:T(8,128)(2,1)} %param.19), kind=kOutput, calls=%fused_computation.106 | convolution fusion | flops 1968384 | bytes 288016 | tf_op jit(solution)/shard_map/dot_general | solution.py:56
  10.7 13.6 %all-gather = f32[4,16,4]{1,2,0:T(4,128)S(1)} all-gather(f32[1,16,4]{1,2,0:T(4,128)S(1)} %bitcast.224), channel_id=1, replica_groups=mesh['dp'=4,'kv'=4,'tp'=2] {'kv'}, dimensions={0}, use_global_device_ids=true | all-gather | bytes 1280 | tf_op jit(solution)/shard_map/all_gather | solution.py:62
  24.8 0.9 transpose_reshape.3
  25.6 1.4 %convolution_convert_fusion.3 = bf16[64,128]{1,0:T(8,128)(2,1)S(1)} fusion(bf16[2048,128]{1,0:T(8,128)(2,1)} %param.23, f32[2048]{0:T(1024)} %param.21, f32[64]{0:T(128)S(1)} %add_rsqrt_fusion.1, bf16[48,2048]{1,0:T(8,128)(2,1)S(1)} %reshape.318, bf16[16,2048]{1,0:T(8,128)(2,1)} %param.19), kind=kOutput, calls=%fused_computation.61 | convolution fusion | flops 34480128 | bytes 811264 | tf_op jit(solution)/shard_map/dot_general | solution.py:51
  27.9 13.1 %all_gather.6 = bf16[64,512]{1,0:T(8,128)(2,1)S(1)} all-gather(bf16[16,512]{1,0:T(8,128)(2,1)S(1)} %slice.44), channel_id=1, replica_groups=mesh['dp'=4,'kv'=4,'tp'=2] {'kv'}, dimensions={0}, use_global_device_ids=true | all-gather | bytes 81920 | tf_op jit(solution)/shard_map/all_gather | solution.py:71
  41.2 4.4 %while.15 = (s32[]{:T(128)}, f32[4,64,1,128]{3,1,2,0:T(8,128)S(1)}, f32[4,64,1]{1,2,0:T(1,128)S(1)}, f32[4,64,1]{1,2,0:T(1,128)S(1)}, bf16[4,64,1,128]{3,1,2,0:T...) while((s32[]{:T(128)}, f32[4,64,1,128]{3,1,2,0:T(8,128)S(1)}, ...), condition=%wide.region_8.9_spmd.clone, body=%wide.region_3.8_spmd.clone.sunk | while | flops 9062274 | bytes 495149 | solution.py:112
  45.7 0.6 copy.73
  46.3 3.4 %all-to-all-start.1 = ((f32[4,16,4]{1,2,0:T(4,128)}), f32[4,16,4]{1,2,0:T(4,128)S(1)}, u32[]{:S(2)}, u32[]{:S(2)}) async-start(f32[4,16,4]{1,2,0:T(4,128)} %copy.73), calls=%async_computation.1 | async-start | bytes 16384 | tf_op jit(solution)/shard_map/all_to_all | solution.py:126
  50.1 0.6 reduce_window_sum.38
  52.1 2.0 %fusion.96 = (f32[12,4,4]{1,2,0:T(4,128)S(1)}, f32[12,1,4,4,512]{4,2,3,0,1:T(4,128)S(1)}) fusion(f32[12,4,512]{2,1,0:T(4,128)S(1)} %copy-done.5, f32[12,4]{1,0:T(8,128)S(1)} %select_reduce_fusion, f32[12,4,4]{1,2,0:T(4,128)S(1)} %copy.78, bf16[12,4,4,128]{3,2,1,0:T(4,128)(2,1)S(1)} %reshape.325, bf16[12,512,1,128]{3,1,2,0:T(8,128)(2,1)} %param.32, ...), kind=kOutput, calls=%fused_computation.119 | convolution fusion | flops 25755456 | bytes 2121408 | tf_op jit(solution)/shard_map/stkgd,spkd->skgtp/dot_general | solution.py:181
  55.7 5.1 %all-to-all-start.2 = ((f32[4,16,4]{1,2,0:T(4,128)}), f32[4,16,4]{1,2,0:T(4,128)S(1)}, u32[]{:S(2)}, u32[]{:S(2)}) async-start(f32[4,16,4]{1,2,0:T(4,128)} %copy.75), calls=%async_computation.2 | async-start | bytes 16384 | tf_op jit(solution)/shard_map/all_to_all | solution.py:133
  60.8 1.8 %fusion.65 = bf16[12,4,1,4,128]{4,1,3,0,2:T(4,128)(2,1)S(1)} fusion(f32[12,4,4,128]{3,2,1,0:T(4,128)S(1)} %convolution_multiply_fusion.2, bf16[12,512,1,128]{3,1,2,0:T(8,128)(2,1)} %param.33, bf16[12,4,4,512]{3,1,2,0:T(4,128)(2,1)S(1)} %get-tuple-element.191, f32[12,4,4]{2,1,0:T(4,128)S(1)} %copy.84), kind=kOutput, calls=%fused_computation.59 | convolution fusion | flops 25239552 | bytes 1917696 | tf_op jit(solution)/shard_map/skgtp,spkd->skgtd/dot_general | solution.py:192
  62.6 0.7 copy.72
  63.3 3.2 %all-to-all-done.2 = f32[4,16,4]{1,2,0:T(4,128)S(1)} async-done(((f32[4,16,4]{1,2,0:T(4,128)}), f32[4,16,4]{1,2,0:T(4,128)S(1)}, u32[]{:S(2)}, u32[]{:S(2)}) %all-to-all-start.2) | async-done | bytes 1056 | tf_op jit(solution)/shard_map/all_to_all | solution.py:133
  66.5 3.3 %all-to-all-start = ((f32[4,16,4,128]{3,1,2,0:T(8,128)}), f32[4,16,4,128]{3,1,2,0:T(8,128)S(1)}, u32[]{:S(2)}, u32[]{:S(2)}) async-start(f32[4,16,4,128]{3,1,2,0:T(8,128)} %copy.72), calls=%async_computation | async-start | bytes 262144 | tf_op jit(solution)/shard_map/all_to_all | solution.py:119
  69.9 5.8 %all-to-all-done = f32[4,16,4,128]{3,1,2,0:T(8,128)S(1)} async-done(((f32[4,16,4,128]{3,1,2,0:T(8,128)}), f32[4,16,4,128]{3,1,2,0:T(8,128)S(1)}, u32[]{:S(2)}, u32[]{:S(2)}) %all-to-all-start) | async-done | bytes 131104 | tf_op jit(solution)/shard_map/all_to_all | solution.py:119
  75.9 1.2 %convolution_convert_fusion = bf16[64,2048]{1,0:T(8,128)(2,1)} fusion(bf16[512,2048]{1,0:T(8,128)(2,1)S(1)} %copy-done, bf16[48,512]{1,0:T(8,128)(2,1)S(1)} %bitcast.214, bf16[16,512]{1,0:T(8,128)(2,1)S(1)} %copy_bitcast_fusion.2), kind=kOutput, calls=%fused_computation.38 | convolution fusion | flops 134479872 | bytes 2424832 | tf_op jit(solution)/shard_map/dot_general | solution.py:205
  77.1 17.4 %all-reduce.2.cloned.1.call-done = bf16[64,2048]{1,0:T(8,128)(2,1)} async-done(((bf16[64,2048]{1,0:T(8,128)(2,1)}), bf16[64,2048]{1,0:T(8,128)(2,1)}) %all-reduce.2.cloned.1.call-update) | async-done | bytes 262160 | tf_op jit(solution)/shard_map/psum | solution.py:206
  94.6 1.1 %fusion.72 = f32[64]{0:T(128)S(1)} fusion(bf16[64,2048]{1,0:T(8,128)(2,1)} %all-reduce.2.cloned.1.call-done), kind=kLoop, calls=%fused_computation.72 | loop fusion | flops 393152 | bytes 262400 | tf_op jit(solution)/shard_map/reduce_sum | solution.py:12
  95.7 1.1 %fusion.74 = bf16[64,2048]{1,0:T(8,128)(2,1)S(1)} fusion(bf16[64,2048]{1,0:T(8,128)(2,1)} %all-reduce.2.cloned.1.call-done, f32[2048]{0:T(1024)S(1)} %copy-done.8, f32[64]{0:T(128)S(1)} %add_rsqrt_fusion), kind=kLoop, calls=%fused_computation.74 | loop fusion | flops 524288 | bytes 532736 | tf_op jit(solution)/shard_map/convert_element_type | solution.py:207
  96.8 0.6 slice.51
  97.4 0.8 reshape.331
  (124 shorter events, 9.5 us)
Async XLA Ops:
  7.2 68.7 %copy-start = (bf16[512,2048]{1,0:T(8,128)(2,1)S(1)}, bf16[512,2048]{1,0:T(8,128)(2,1)}, u32[]{:S(2)}) copy-start(bf16[512,2048]{1,0:T(8,128)(2,1)} %param.27) | copy-start | bytes 6291460
  7.2 19.8 %copy-start.4 = (bf16[16,2048]{1,0:T(8,128)(2,1)S(1)}, bf16[16,2048]{1,0:T(8,128)(2,1)}, u32[]{:S(2)}) copy-start(bf16[16,2048]{1,0:T(8,128)(2,1)} %param.19) | copy-start | bytes 196612
  7.2 19.8 %copy-start.7 = (f32[2048]{0:T(1024)S(1)}, f32[2048]{0:T(1024)}, u32[]{:S(2)}) copy-start(f32[2048]{0:T(1024)} %param.21) | copy-start | bytes 24580
  7.2 19.8 %copy-start.10 = (bf16[2048,128]{1,0:T(8,128)(2,1)S(1)}, bf16[2048,128]{1,0:T(8,128)(2,1)}, u32[]{:S(2)}) copy-start(bf16[2048,128]{1,0:T(8,128)(2,1)} %param.24) | copy-start | bytes 1572868
  24.8 2.6 %copy-start.1 = (bf16[2048,512]{1,0:T(8,128)(2,1)S(1)}, bf16[2048,512]{1,0:T(8,128)(2,1)}, u32[]{:S(2)}) copy-start(bf16[2048,512]{1,0:T(8,128)(2,1)} %param.22) | copy-start | bytes 6291460
  27.0 14.2 %copy-start.2 = (bf16[256,1,128]{2,0,1:T(8,128)(2,1)S(1)}, bf16[256,1,128]{2,0,1:T(8,128)(2,1)}, u32[]{:S(2)}) copy-start(bf16[256,1,128]{2,0,1:T(8,128)(2,1)} %param.29) | copy-start | bytes 196612
  27.0 14.2 %copy-start.3 = (bf16[256,1,128]{2,0,1:T(8,128)(2,1)S(1)}, bf16[256,1,128]{2,0,1:T(8,128)(2,1)}, u32[]{:S(2)}) copy-start(bf16[256,1,128]{2,0,1:T(8,128)(2,1)} %param.30) | copy-start | bytes 196612
  27.4 22.5 %copy-start.6 = (bf16[64,128]{1,0:T(8,128)(2,1)}, bf16[64,128]{1,0:T(8,128)(2,1)S(1)}, u32[]{:S(2)}) copy-start(bf16[64,128]{1,0:T(8,128)(2,1)S(1)} %convolution_convert_fusion.2) | copy-start | bytes 49156
  27.9 21.8 %copy-start.9 = (s32[12]{0:T(128)S(1)}, s32[12]{0:T(128)}, u32[]{:S(2)}) copy-start(s32[12]{0:T(128)} %param.35) | copy-start | bytes 148
  41.2 10.8 %copy-start.5 = (f32[12,4,512]{2,1,0:T(4,128)S(1)}, f32[12,4,512]{2,1,0:T(4,128)}, u32[]{:S(2)}) copy-start(f32[12,4,512]{2,1,0:T(4,128)} %param.34) | copy-start | bytes 294916
  46.3 9.4 %all-to-all-start.1 = ((f32[4,16,4]{1,2,0:T(4,128)}), f32[4,16,4]{1,2,0:T(4,128)S(1)}, u32[]{:S(2)}, u32[]{:S(2)}) async-start(f32[4,16,4]{1,2,0:T(4,128)} %copy.73), calls=%async_computation.1 | async-start | bytes 16384 | tf_op jit(solution)/shard_map/all_to_all | solution.py:126
  50.1 4.6 %slice-start = ((bf16[64,128]{1,0:T(8,128)(2,1)}), bf16[48,128]{1,0:T(8,128)(2,1)S(1)}, s32[]{:S(2)}) async-start(bf16[64,128]{1,0:T(8,128)(2,1)} %copy-done.6), calls=%async_computation.4 | async-start | bytes 24576 | tf_op jit(solution)/shard_map/slice | solution.py:148
  55.7 10.8 %all-to-all-start.2 = ((f32[4,16,4]{1,2,0:T(4,128)}), f32[4,16,4]{1,2,0:T(4,128)S(1)}, u32[]{:S(2)}, u32[]{:S(2)}) async-start(f32[4,16,4]{1,2,0:T(4,128)} %copy.75), calls=%async_computation.2 | async-start | bytes 16384 | tf_op jit(solution)/shard_map/all_to_all | solution.py:133
  62.6 33.1 %copy-start.8 = (f32[2048]{0:T(1024)S(1)}, f32[2048]{0:T(1024)}, u32[]{:S(2)}) copy-start(f32[2048]{0:T(1024)} %param.28) | copy-start | bytes 24580
  66.5 9.2 %all-to-all-start = ((f32[4,16,4,128]{3,1,2,0:T(8,128)}), f32[4,16,4,128]{3,1,2,0:T(8,128)S(1)}, u32[]{:S(2)}, u32[]{:S(2)}) async-start(f32[4,16,4,128]{3,1,2,0:T(8,128)} %copy.72), calls=%async_computation | async-start | bytes 262144 | tf_op jit(solution)/shard_map/all_to_all | solution.py:119
  69.8 24.7 %all-reduce.2.cloned.1.call-start = ((), (), s32[]{:S(2)}) async-start(), calls=%async_computation.3 | async-start | bytes 524288 | tf_op jit(solution)/shard_map/psum | solution.py:206
Sparse Core Ops, SparseCore 0:
  77.2 17.2 all-reduce.1
where the time goes:
time: 106 us; the launch traced here: 105 us
  blocking collectives  26.8 us (25%)
  waiting for transfers between devices  26.5 us (25%)
  between operations  14.4 us (14%)
  matrix products  12.2 us (12%)
  starting transfers between devices  11.9 us (11%)
  local copies, waits for them, and re-layouts  7.15 us (7%)
  other arithmetic  6.01 us (6%)
    psum x1, waiting for transfers between devices, body(): lax.psum(partial_rows.astype(jnp.bfloat16), 'tp').astype(jnp.float32)  17.4 us
    all_gather x1, blocking collectives, body(): gathered_run = lax.all_gather(local_run, 'kv', axis=0, tiled=True)  13.6 us
    all_gather x1, blocking collectives, body(): shard_queries = lax.all_gather(piece_queries, 'kv', axis=0, tiled=True)  13.1 us
    all_to_all x1, waiting for transfers between devices, body(): lax.all_to_all(group_out.reshape(kv_count, piece_rows, heads_local, head_...  5.81 us
    all_to_all x1, starting transfers between devices, body(): lax.all_to_all(group_total.reshape(kv_count, piece_rows, heads_local), 'k...  5.09 us
    all_to_all x1, starting transfers between devices, body(): lax.all_to_all(group_top.reshape(kv_count, piece_rows, heads_local), 'kv'...  3.44 us
    all_to_all x1, starting transfers between devices, body(): lax.all_to_all(group_out.reshape(kv_count, piece_rows, heads_local, head_...  3.33 us
    all_to_all x1, waiting for transfers between devices, body(): lax.all_to_all(group_total.reshape(kv_count, piece_rows, heads_local), 'k...  3.19 us
  transfers between devices with their start and end apart: 4, of which 3 were waited for; matrix products, arithmetic and copies ran while one was open for 8% of the time, Pallas kernels for 0%

commit v1 on v0

--- a/solution.py
+++ b/solution.py
@@ -68,7 +68,8 @@
     key_place = position * piece_rows + jnp.arange(piece_rows)
     gate_groups = jnp.moveaxis(past_gate.reshape(kv_local, group_size, -1), 1, 0)
     own_groups = jnp.moveaxis(own_run.reshape(piece_rows, kv_local, group_size), 2, 0)
-    shard_queries = lax.all_gather(piece_queries, "kv", axis=0, tiled=True)
+    sent = jnp.stack([piece_queries] * lax.axis_size("kv"))
+    shard_queries = jnp.concatenate(lax.all_to_all(sent, "kv", 0, 0), axis=0)
     row_count = shard_queries.shape[0]
     query_groups = jnp.moveaxis(
         shard_queries.reshape(row_count, kv_local, group_size, head_dim), 2, 0

time: 106 us -> 101 us (0.953)
  blocking collectives: 26.8 us -> 12.5 us
  waiting for transfers between devices: 26.5 us -> 30.9 us
  starting transfers between devices: 11.9 us -> 16.2 us
    all_gather x1 -> x0, blocking collectives: 13.1 us -> none  [body(): shard_queries = lax.all_gather(piece_queries, 'kv', axis=0, tiled=True)]
    all_to_all x0 -> x1, starting transfers between devices: none -> 6.34 us  [body(): shard_queries = jnp.concatenate(lax.all_to_all(sent, 'kv', 0, 0), axis=0)]
    all_to_all x1, waiting for transfers between devices: 0.01 us -> 4.58 us  [body(): lax.all_to_all(group_top.reshape(kv_count, piece_rows, heads_local), 'kv'...]
    all_to_all x1, starting transfers between devices: 5.09 us -> 3.25 us  [body(): lax.all_to_all(group_total.reshape(kv_count, piece_rows, heads_local), 'k...]
    dot_general x1, matrix products: 0.52 us -> 2.18 us  [body(): jnp.dot(normed, query_weight, preferred_element_type=jnp.float32)]
    all_gather x1, blocking collectives: 13.6 us -> 12.5 us  [body(): gathered_run = lax.all_gather(local_run, 'kv', axis=0, tiled=True)]
    dot_general x1, matrix products: 1.37 us -> 0.29 us  [body(): jnp.dot(normed, key_weight, preferred_element_type=jnp.float32)]
  transfers between devices with their start and end apart: 4 -> 5, of which waited for: 3 -> 4; matrix products, arithmetic and copies ran while one was open for 8% -> 11% of each run, Pallas kernels for 0% -> 0%
where the time goes in v1:
time: 101 us; the launch traced here: 100 us
  waiting for transfers between devices  30.9 us (31%)
  starting transfers between devices  16.2 us (16%)
  between operations  14.5 us (14%)
  matrix products  12.9 us (13%)
  blocking collectives  12.5 us (12%)
  local copies, waits for them, and re-layouts  6.94 us (7%)
  other arithmetic  6.01 us (6%)
    psum x1, waiting for transfers between devices, body(): lax.psum(partial_rows.astype(jnp.bfloat16), 'tp').astype(jnp.float32)  17.4 us
    all_gather x1, blocking collectives, body(): gathered_run = lax.all_gather(local_run, 'kv', axis=0, tiled=True)  12.5 us
    all_to_all x1, starting transfers between devices, body(): shard_queries = jnp.concatenate(lax.all_to_all(sent, 'kv', 0, 0), axis=0)  6.34 us
    all_to_all x1, waiting for transfers between devices, body(): lax.all_to_all(group_out.reshape(kv_count, piece_rows, heads_local, head_...  5.81 us
    all_to_all x1, waiting for transfers between devices, body(): lax.all_to_all(group_top.reshape(kv_count, piece_rows, heads_local), 'kv'...  4.58 us
    all_to_all x1, starting transfers between devices, body(): lax.all_to_all(group_out.reshape(kv_count, piece_rows, heads_local, head_...  3.33 us
    all_to_all x1, starting transfers between devices, body(): lax.all_to_all(group_top.reshape(kv_count, piece_rows, heads_local), 'kv'...  3.25 us
    all_to_all x1, starting transfers between devices, body(): lax.all_to_all(group_total.reshape(kv_count, piece_rows, heads_local), 'k...  3.25 us
  transfers between devices with their start and end apart: 5, of which 4 were waited for; matrix products, arithmetic and copies ran while one was open for 11% of the time, Pallas kernels for 0%

profile of v1, /device:TPU:0, one launch (start us, length us, event | category | flops | bytes accessed | tf_op | source)
XLA Modules:
  0.0 100.2 jit_solution(10004748126833677245)
XLA Ops:
  7.2 1.1 %reshape.317 = bf16[48,2048]{1,0:T(8,128)(2,1)S(1)} reshape(bf16[12,4,2048]{2,1,0:T(4,128)(2,1)} %param.20) | data formatting | bytes 393216 | tf_op jit(solution)/shard_map/reshape | solution.py:47
  8.4 1.0 fusion.69
  9.4 2.2 %convolution_convert_fusion.1 = bf16[64,512]{1,0:T(8,128)(2,1)S(1)} fusion(bf16[2048,512]{1,0:T(8,128)(2,1)} %param.22, f32[2048]{0:T(1024)} %param.21, f32[64]{0:T(128)S(1)} %add_rsqrt_fusion.1, bf16[48,2048]{1,0:T(8,128)(2,1)S(1)} %reshape.317, bf16[16,2048]{1,0:T(8,128)(2,1)} %param.19), kind=kOutput, calls=%fused_computation.54 | convolution fusion | flops 135168000 | bytes 2433280 | tf_op jit(solution)/shard_map/dot_general | solution.py:50
  11.6 0.6 stack.2
  12.2 6.3 %all-to-all-start = ((bf16[4,16,512]{2,1,0:T(8,128)(2,1)}), bf16[4,16,512]{2,1,0:T(8,128)(2,1)S(1)}, u32[]{:S(2)}, u32[]{:S(2)}) async-start(bf16[4,16,512]{2,1,0:T(8,128)(2,1)} %stack.2), calls=%async_computation | async-start | bytes 131072 | tf_op jit(solution)/shard_map/all_to_all | solution.py:72
  19.3 12.5 %all-gather = f32[4,16,4]{1,2,0:T(4,128)S(1)} all-gather(f32[1,16,4]{1,2,0:T(4,128)S(1)} %bitcast.222), channel_id=1, replica_groups=mesh['dp'=4,'kv'=4,'tp'=2] {'kv'}, dimensions={0}, use_global_device_ids=true | all-gather | bytes 1280 | tf_op jit(solution)/shard_map/all_gather | solution.py:62
  32.5 1.3 %convolution_convert_fusion.2 = bf16[64,128]{1,0:T(8,128)(2,1)S(1)} fusion(bf16[2048,128]{1,0:T(8,128)(2,1)} %param.24, f32[2048]{0:T(1024)S(1)} %copy-done.6, f32[64]{0:T(128)S(1)} %add_rsqrt_fusion.1, bf16[48,2048]{1,0:T(8,128)(2,1)S(1)} %reshape.317, bf16[16,2048]{1,0:T(8,128)(2,1)S(1)} %copy-done.3), kind=kOutput, calls=%fused_computation.60 | convolution fusion | flops 34480128 | bytes 811264 | tf_op jit(solution)/shard_map/dot_general | solution.py:52
  34.1 0.6 reduce_window_sum.38
  36.1 2.0 %fusion.96 = (f32[12,4,4]{1,2,0:T(4,128)S(1)}, f32[12,1,4,4,512]{4,2,3,0,1:T(4,128)S(1)}) fusion(f32[12,4,512]{2,1,0:T(4,128)S(1)} %copy-done.4, f32[12,4]{1,0:T(8,128)S(1)} %select_reduce_fusion, f32[12,4,4]{1,2,0:T(4,128)S(1)} %copy.77, bf16[12,4,4,128]{3,2,1,0:T(4,128)(2,1)S(1)} %reshape.323, bf16[12,512,1,128]{3,1,2,0:T(8,128)(2,1)} %param.32, ...), kind=kOutput, calls=%fused_computation.118 | convolution fusion | flops 25755456 | bytes 2121408 | tf_op jit(solution)/shard_map/stkgd,spkd->skgtp/dot_general | solution.py:182
  38.8 4.4 %while.15 = (s32[]{:T(128)}, f32[4,64,1,128]{3,1,2,0:T(8,128)S(1)}, f32[4,64,1]{1,2,0:T(1,128)S(1)}, f32[4,64,1]{1,2,0:T(1,128)S(1)}, bf16[4,64,1,128]{3,1,2,0:T...) while((s32[]{:T(128)}, f32[4,64,1,128]{3,1,2,0:T(8,128)S(1)}, ...), condition=%wide.region_8.9_spmd.clone, body=%wide.region_3.8_spmd.clone.sunk | while | flops 9062274 | bytes 495149 | solution.py:113
  44.0 3.2 %all-to-all-start.2 = ((f32[4,16,4]{1,2,0:T(4,128)}), f32[4,16,4]{1,2,0:T(4,128)S(1)}, u32[]{:S(2)}, u32[]{:S(2)}) async-start(f32[4,16,4]{1,2,0:T(4,128)} %copy.72), calls=%async_computation.2 | async-start | bytes 16384 | tf_op jit(solution)/shard_map/all_to_all | solution.py:127
  48.2 4.6 %all-to-all-done.2 = f32[4,16,4]{1,2,0:T(4,128)S(1)} async-done(((f32[4,16,4]{1,2,0:T(4,128)}), f32[4,16,4]{1,2,0:T(4,128)S(1)}, u32[]{:S(2)}, u32[]{:S(2)}) %all-to-all-start.2) | async-done | bytes 1056 | tf_op jit(solution)/shard_map/all_to_all | solution.py:127
  52.8 3.2 %all-to-all-start.3 = ((f32[4,16,4]{1,2,0:T(4,128)}), f32[4,16,4]{1,2,0:T(4,128)S(1)}, u32[]{:S(2)}, u32[]{:S(2)}) async-start(f32[4,16,4]{1,2,0:T(4,128)} %copy.74), calls=%async_computation.3 | async-start | bytes 16384 | tf_op jit(solution)/shard_map/all_to_all | solution.py:134
  56.1 1.8 %fusion.65 = bf16[12,4,1,4,128]{4,1,3,0,2:T(4,128)(2,1)S(1)} fusion(f32[12,4,4,128]{3,2,1,0:T(4,128)S(1)} %convolution_multiply_fusion.2, bf16[12,512,1,128]{3,1,2,0:T(8,128)(2,1)} %param.33, bf16[12,4,4,512]{3,1,2,0:T(4,128)(2,1)S(1)} %get-tuple-element.191, f32[12,4,4]{2,1,0:T(4,128)S(1)} %copy.83), kind=kOutput, calls=%fused_computation.59 | convolution fusion | flops 25239552 | bytes 1917696 | tf_op jit(solution)/shard_map/skgtp,spkd->skgtd/dot_general | solution.py:193
  57.9 0.7 copy.71
  58.6 3.0 %all-to-all-done.3 = f32[4,16,4]{1,2,0:T(4,128)S(1)} async-done(((f32[4,16,4]{1,2,0:T(4,128)}), f32[4,16,4]{1,2,0:T(4,128)S(1)}, u32[]{:S(2)}, u32[]{:S(2)}) %all-to-all-start.3) | async-done | bytes 1056 | tf_op jit(solution)/shard_map/all_to_all | solution.py:134
  61.6 3.3 %all-to-all-start.1 = ((f32[4,16,4,128]{3,1,2,0:T(8,128)}), f32[4,16,4,128]{3,1,2,0:T(8,128)S(1)}, u32[]{:S(2)}, u32[]{:S(2)}) async-start(f32[4,16,4,128]{3,1,2,0:T(8,128)} %copy.71), calls=%async_computation.1 | async-start | bytes 262144 | tf_op jit(solution)/shard_map/all_to_all | solution.py:120
  65.0 5.8 %all-to-all-done.1 = f32[4,16,4,128]{3,1,2,0:T(8,128)S(1)} async-done(((f32[4,16,4,128]{3,1,2,0:T(8,128)}), f32[4,16,4,128]{3,1,2,0:T(8,128)S(1)}, u32[]{:S(2)}, u32[]{:S(2)}) %all-to-all-start.1) | async-done | bytes 131104 | tf_op jit(solution)/shard_map/all_to_all | solution.py:120
  71.0 1.2 %convolution_convert_fusion = bf16[64,2048]{1,0:T(8,128)(2,1)} fusion(bf16[512,2048]{1,0:T(8,128)(2,1)S(1)} %copy-done, bf16[48,512]{1,0:T(8,128)(2,1)S(1)} %bitcast.212, bf16[16,512]{1,0:T(8,128)(2,1)S(1)} %copy_bitcast_fusion.1), kind=kOutput, calls=%fused_computation.38 | convolution fusion | flops 134479872 | bytes 2424832 | tf_op jit(solution)/shard_map/dot_general | solution.py:206
  72.2 17.4 %all-reduce.2.cloned.1.call-done = bf16[64,2048]{1,0:T(8,128)(2,1)} async-done(((bf16[64,2048]{1,0:T(8,128)(2,1)}), bf16[64,2048]{1,0:T(8,128)(2,1)}) %all-reduce.2.cloned.1.call-update) | async-done | bytes 262160 | tf_op jit(solution)/shard_map/psum | solution.py:207
  89.7 1.1 %fusion.72 = f32[64]{0:T(128)S(1)} fusion(bf16[64,2048]{1,0:T(8,128)(2,1)} %all-reduce.2.cloned.1.call-done), kind=kLoop, calls=%fused_computation.72 | loop fusion | flops 393152 | bytes 262400 | tf_op jit(solution)/shard_map/reduce_sum | solution.py:12
  90.8 1.1 %fusion.74 = bf16[64,2048]{1,0:T(8,128)(2,1)S(1)} fusion(bf16[64,2048]{1,0:T(8,128)(2,1)} %all-reduce.2.cloned.1.call-done, f32[2048]{0:T(1024)S(1)} %copy-done.7, f32[64]{0:T(128)S(1)} %add_rsqrt_fusion), kind=kLoop, calls=%fused_computation.74 | loop fusion | flops 524288 | bytes 532736 | tf_op jit(solution)/shard_map/convert_element_type | solution.py:208
  91.9 0.6 slice.51
  92.6 0.8 reshape.329
  (130 shorter events, 9.8 us)
Async XLA Ops:
  7.2 63.9 %copy-start = (bf16[512,2048]{1,0:T(8,128)(2,1)S(1)}, bf16[512,2048]{1,0:T(8,128)(2,1)}, u32[]{:S(2)}) copy-start(bf16[512,2048]{1,0:T(8,128)(2,1)} %param.27) | copy-start | bytes 6291460
  7.2 11.5 %copy-start.3 = (bf16[16,2048]{1,0:T(8,128)(2,1)S(1)}, bf16[16,2048]{1,0:T(8,128)(2,1)}, u32[]{:S(2)}) copy-start(bf16[16,2048]{1,0:T(8,128)(2,1)} %param.19) | copy-start | bytes 196612
  7.2 11.5 %copy-start.6 = (f32[2048]{0:T(1024)S(1)}, f32[2048]{0:T(1024)}, u32[]{:S(2)}) copy-start(f32[2048]{0:T(1024)} %param.21) | copy-start | bytes 24580
  7.2 11.4 %copy-start.9 = (s32[12]{0:T(128)S(1)}, s32[12]{0:T(128)}, u32[]{:S(2)}) copy-start(s32[12]{0:T(128)} %param.35) | copy-start | bytes 148
  7.2 11.5 %copy-start.12 = (f32[4]{0:T(128)S(1)}, f32[4]{0:T(128)}, u32[]{:S(2)}) copy-start(f32[4]{0:T(128)} %param.26) | copy-start | bytes 52
  7.2 11.5 %copy-start.11 = (bf16[2048,4]{0,1:T(4,128)(2,1)S(1)}, bf16[2048,4]{0,1:T(4,128)(2,1)}, u32[]{:S(2)}) copy-start(bf16[2048,4]{0,1:T(4,128)(2,1)} %param.25) | copy-start | bytes 49156
  7.2 24.9 %copy-start.10 = (bf16[2048,128]{1,0:T(8,128)(2,1)S(1)}, bf16[2048,128]{1,0:T(8,128)(2,1)}, u32[]{:S(2)}) copy-start(bf16[2048,128]{1,0:T(8,128)(2,1)} %param.23) | copy-start | bytes 1572868
  11.6 22.3 %copy-start.8 = (f32[4,256]{1,0:T(4,128)S(1)}, f32[4,256]{1,0:T(4,128)}, u32[]{:S(2)}) copy-start(f32[4,256]{1,0:T(4,128)} %param.31) | copy-start | bytes 12292
  12.2 26.5 %all-to-all-start = ((bf16[4,16,512]{2,1,0:T(8,128)(2,1)}), bf16[4,16,512]{2,1,0:T(8,128)(2,1)S(1)}, u32[]{:S(2)}, u32[]{:S(2)}) async-start(bf16[4,16,512]{2,1,0:T(8,128)(2,1)} %stack.2), calls=%async_computation | async-start | bytes 131072 | tf_op jit(solution)/shard_map/all_to_all | solution.py:72
  18.6 17.4 %copy-start.4 = (f32[12,4,512]{2,1,0:T(4,128)S(1)}, f32[12,4,512]{2,1,0:T(4,128)}, u32[]{:S(2)}) copy-start(f32[12,4,512]{2,1,0:T(4,128)} %param.34) | copy-start | bytes 294916
  33.8 4.7 %copy-start.5 = (bf16[64,128]{1,0:T(8,128)(2,1)}, bf16[64,128]{1,0:T(8,128)(2,1)S(1)}, u32[]{:S(2)}) copy-start(bf16[64,128]{1,0:T(8,128)(2,1)S(1)} %convolution_convert_fusion.2) | copy-start | bytes 49156
  34.9 4.0 %copy-start.1 = (bf16[256,1,128]{2,0,1:T(8,128)(2,1)S(1)}, bf16[256,1,128]{2,0,1:T(8,128)(2,1)}, u32[]{:S(2)}) copy-start(bf16[256,1,128]{2,0,1:T(8,128)(2,1)} %param.29) | copy-start | bytes 196612
  34.9 4.0 %copy-start.2 = (bf16[256,1,128]{2,0,1:T(8,128)(2,1)S(1)}, bf16[256,1,128]{2,0,1:T(8,128)(2,1)}, u32[]{:S(2)}) copy-start(bf16[256,1,128]{2,0,1:T(8,128)(2,1)} %param.30) | copy-start | bytes 196612
  38.5 8.7 %slice-start = ((bf16[64,128]{1,0:T(8,128)(2,1)}), bf16[48,128]{1,0:T(8,128)(2,1)S(1)}, s32[]{:S(2)}) async-start(bf16[64,128]{1,0:T(8,128)(2,1)} %copy-done.5), calls=%async_computation.5 | async-start | bytes 24576 | tf_op jit(solution)/shard_map/slice | solution.py:149
  44.0 8.8 %all-to-all-start.2 = ((f32[4,16,4]{1,2,0:T(4,128)}), f32[4,16,4]{1,2,0:T(4,128)S(1)}, u32[]{:S(2)}, u32[]{:S(2)}) async-start(f32[4,16,4]{1,2,0:T(4,128)} %copy.72), calls=%async_computation.2 | async-start | bytes 16384 | tf_op jit(solution)/shard_map/all_to_all | solution.py:127
  52.8 8.8 %all-to-all-start.3 = ((f32[4,16,4]{1,2,0:T(4,128)}), f32[4,16,4]{1,2,0:T(4,128)S(1)}, u32[]{:S(2)}, u32[]{:S(2)}) async-start(f32[4,16,4]{1,2,0:T(4,128)} %copy.74), calls=%async_computation.3 | async-start | bytes 16384 | tf_op jit(solution)/shard_map/all_to_all | solution.py:134
  57.8 33.0 %copy-start.7 = (f32[2048]{0:T(1024)S(1)}, f32[2048]{0:T(1024)}, u32[]{:S(2)}) copy-start(f32[2048]{0:T(1024)} %param.28) | copy-start | bytes 24580
  61.6 9.2 %all-to-all-start.1 = ((f32[4,16,4,128]{3,1,2,0:T(8,128)}), f32[4,16,4,128]{3,1,2,0:T(8,128)S(1)}, u32[]{:S(2)}, u32[]{:S(2)}) async-start(f32[4,16,4,128]{3,1,2,0:T(8,128)} %copy.71), calls=%async_computation.1 | async-start | bytes 262144 | tf_op jit(solution)/shard_map/all_to_all | solution.py:120
  64.9 24.7 %all-reduce.2.cloned.1.call-start = ((), (), s32[]{:S(2)}) async-start(), calls=%async_computation.4 | async-start | bytes 524288 | tf_op jit(solution)/shard_map/psum | solution.py:207
Sparse Core Ops, SparseCore 0:
  72.4 17.2 all-reduce.1
